TPU v7x, 32 devices: a whole 2x2x4 slice. The times are simulated.
32 devices in a mesh: sp: 8 (over z, y), tp: 4 (over x, core).
Axes of the slice: x: 2, y: 2, z: 4, core: 2. Of those that a mesh axis runs over, the one named last changes fastest.
Arguments:
- tokens: bfloat16 [2048, 4096], P(('sp', 'tp')), may hold values from -6 to 6
- norm_gain: float32 [4096], replicated, may hold values from 0.1 to 1.9
- w_query: bfloat16 [4096, 1024], P(None, 'tp'), may hold values from -0.25 to 0.25
- w_key: bfloat16 [4096, 512], P(None, 'tp'), may hold values from -0.09375 to 0.09375
- w_value: bfloat16 [4096, 512], P(None, 'tp'), may hold values from -0.09375 to 0.09375
- score_shift: float32 [8], P('tp'), may hold values from -15 to -8
- w_conv_b: bfloat16 [4096, 1024], P(None, 'tp'), may hold values from -0.09375 to 0.09375
- w_conv_c: bfloat16 [4096, 1024], P(None, 'tp'), may hold values from -0.09375 to 0.09375
- w_conv_u: bfloat16 [4096, 1024], P(None, 'tp'), may hold values from -0.09375 to 0.09375
- conv_kernel: float32 [3, 1024], P(None, 'tp'), may hold values from -3.5 to 3.5
- w_out_att: bfloat16 [4096, 1024], P('sp', 'tp'), may hold values from -0.75 to 0.75
- w_out_conv: bfloat16 [4096, 1024], P('sp', 'tp'), may hold values from -0.1875 to 0.1875
Outputs:
- mixed: bfloat16 [2048, 4096], P(('sp', 'tp'))
- log_weight: float32 [2048, 8], P('sp', 'tp')
All inputs are finite; a program needn't handle non-finite values.
Results may differ from a plain program's by a relative error of at most 0.017.
Values may be sent and summed in bfloat16 or wider, within the bound.
A program may use at most 128 MiB of HBM per device.

v0:
```python
import jax
import jax.numpy as jnp
from jax import lax
from jax.sharding import PartitionSpec as P

HEAD_DIM = 128
CONV_K = 3
KEY_BLOCK = 1024


def swapped(block, axis, stride):
    count = lax.axis_size(axis)
    route = []
    for low in range(count):
        high = low | 1 << stride
        if high != low and high < count:
            route += [(low, high), (high, low)]
    return lax.ppermute(block, axis, route)


def shifted(value, axis, steps):
    count = lax.axis_size(axis)
    leading, last = (max(0, -steps), min(count, count - steps))
    return lax.ppermute(value, axis, [(source, source + steps) for source in range(leading, last)])


def normalize(tokens, norm_gain):
    widened = tokens.astype(jnp.float32)
    inverse = lax.rsqrt(jnp.mean(widened * widened, axis=-1, keepdims=True) + 1e-06)
    return (widened * inverse * norm_gain).astype(jnp.bfloat16)


def block_terms(grouped_q, key_block, value_block, shifts, query_pos, key_first):
    scores = jnp.einsum("qhgd,khd->qhgk", grouped_q, key_block, preferred_element_type=jnp.float32)
    scores = scores * HEAD_DIM ** (-0.5) + shifts[None, :, :, None]
    key_pos = key_first + jnp.arange(KEY_BLOCK, dtype=jnp.int32)
    causal = key_pos[None, None, None, :] < query_pos[:, None, None, None]
    soft = jnp.where(causal, jax.nn.softplus(scores), 0.0)
    after_sum = lax.cumsum(soft, axis=3, reverse=True) - soft
    relative = jnp.where(causal, jnp.exp(jax.nn.log_sigmoid(scores) - after_sum), 0.0).astype(
        jnp.bfloat16
    )
    partial_value = jnp.einsum(
        "qhgk,khd->qhgd", relative, value_block, preferred_element_type=jnp.float32
    )
    return (partial_value, jnp.sum(soft, axis=3))


def attend(grouped_q, query_pos, key_whole, value_whole, shifts):
    row_count, kv_local, grouping, head_size = grouped_q.shape
    last_block = jnp.max(query_pos) // KEY_BLOCK

    def visit(step, carry):
        accum, suffix = carry
        block_no = last_block - step
        key_first = block_no * KEY_BLOCK
        key_block = lax.dynamic_slice_in_dim(key_whole, key_first, KEY_BLOCK, 0).reshape(
            KEY_BLOCK, kv_local, head_size
        )
        value_block = lax.dynamic_slice_in_dim(value_whole, key_first, KEY_BLOCK, 0).reshape(
            KEY_BLOCK, kv_local, head_size
        )
        partial_value, total = block_terms(
            grouped_q, key_block, value_block, shifts, query_pos, key_first
        )
        accum = accum + jnp.exp(-suffix)[..., None] * partial_value
        return (accum, suffix + total)

    start = (
        jnp.zeros((row_count, kv_local, grouping, head_size), jnp.float32),
        jnp.zeros((row_count, kv_local, grouping), jnp.float32),
    )
    accum, suffix = lax.fori_loop(0, last_block + 1, visit, start)
    return (
        accum.reshape(row_count, kv_local * grouping * head_size),
        suffix.reshape(row_count, kv_local * grouping),
    )


def mirror_queries(payload):
    for bit in range(lax.axis_size("sp").bit_length() - 1):
        payload = swapped(payload, "sp", bit)
    return payload


def mirror_results(payload):
    for bit in range(lax.axis_size("sp").bit_length() - 1):
        payload = (
            swapped(payload[0].astype(jnp.bfloat16), "sp", bit).astype(jnp.float32),
            swapped(payload[1].astype(jnp.bfloat16), "sp", bit).astype(jnp.float32),
        )
    return payload


def local(
    tokens,
    norm_gain,
    w_query,
    w_key,
    w_value,
    score_shift,
    w_conv_b,
    w_conv_c,
    w_conv_u,
    conv_kernel,
    w_out_att,
    w_out_conv,
):
    weights = (w_query, w_key, w_value, w_conv_b, w_conv_c, w_conv_u)

    def project(rows_in):
        normed = normalize(rows_in, norm_gain)
        return jnp.concatenate(
            [
                jnp.dot(normed, weight, preferred_element_type=jnp.float32).astype(jnp.bfloat16)
                for weight in weights
            ],
            axis=1,
        )

    projected = project(lax.all_gather(tokens, "tp", axis=0, tiled=True))
    widths = [weight.shape[1] for weight in weights]
    edges = [0]
    for width in widths:
        edges.append(edges[-1] + width)
    queries, keys, values, gate_b, gate_c, inputs_u = [
        projected[:, edges[pos] : edges[pos + 1]] for pos in range(6)
    ]
    tok_count = projected.shape[0]
    conv_local = gate_b.shape[1]
    products = (gate_c.astype(jnp.float32) * inputs_u.astype(jnp.float32)).astype(jnp.bfloat16)
    previous = shifted(products[tok_count - (CONV_K - 1) :], "sp", 1)
    key_whole, value_whole = (
        lax.all_gather(keys, "sp", axis=0, tiled=True),
        lax.all_gather(values, "sp", axis=0, tiled=True),
    )
    local_heads = queries.shape[1] // HEAD_DIM
    kv_local = keys.shape[1] // HEAD_DIM
    grouping = local_heads // kv_local
    shifts = score_shift.reshape(kv_local, grouping)
    sp_count = lax.axis_size("sp")
    sp_index = lax.axis_index("sp")
    half = tok_count // 2
    own_q = queries[:half].reshape(half, kv_local, grouping, HEAD_DIM)
    own_pos = sp_index * tok_count + jnp.arange(half, dtype=jnp.int32)
    own_att, own_sums = attend(own_q, own_pos, key_whole, value_whole, shifts)
    other_q = mirror_queries(queries[half:]).reshape(tok_count - half, kv_local, grouping, HEAD_DIM)
    other_pos = (
        (sp_count - 1 - sp_index) * tok_count + half + jnp.arange(tok_count - half, dtype=jnp.int32)
    )
    other_att, other_sums = attend(other_q, other_pos, key_whole, value_whole, shifts)
    back_att, back_sums = mirror_results((other_att, other_sums))
    attended_f = jnp.concatenate([own_att, back_att], axis=0)
    sums_all = jnp.concatenate([own_sums, back_sums], axis=0)
    attended = attended_f.astype(jnp.bfloat16)
    log_weight = jnp.log(jnp.maximum(-jnp.expm1(-sums_all), 0.05))
    extended = jnp.concatenate([previous, products], axis=0)
    summed = jnp.zeros((tok_count, conv_local), jnp.float32)
    for tap in range(CONV_K):
        summed = summed + conv_kernel[tap][None, :] * extended[tap : tap + tok_count].astype(
            jnp.float32
        )
    convolved = (gate_b.astype(jnp.float32) * summed).astype(jnp.bfloat16)
    contract = (((1,), (1,)), ((), ()))
    pieces = lax.all_gather((w_out_att, w_out_conv), "sp", axis=0, tiled=True)
    result = lax.dot_general(attended, pieces[0], contract, preferred_element_type=jnp.float32)
    share = result + lax.dot_general(
        convolved, pieces[1], contract, preferred_element_type=jnp.float32
    )
    rounded = share.astype(jnp.bfloat16).astype(jnp.float32)
    mixed = lax.psum_scatter(rounded.astype(jnp.bfloat16), "tp", scatter_dimension=0, tiled=True)
    return (mixed, log_weight)


def solution(mesh):
    return jax.shard_map(
        local,
        mesh=mesh,
        in_specs=(
            P(("sp", "tp"), None),
            P(),
            P(None, "tp"),
            P(None, "tp"),
            P(None, "tp"),
            P("tp"),
            P(None, "tp"),
            P(None, "tp"),
            P(None, "tp"),
            P(None, "tp"),
            P("sp", "tp"),
            P("sp", "tp"),
        ),
        out_specs=(P(("sp", "tp"), None), P("sp", "tp")),
        check_vma=False,
    )
```

profile of v0, /device:TPU:0, one launch (start us, length us, event | category | flops | bytes accessed | tf_op | source)
XLA Modules:
  0.0 195.4 jit_solution(12022105615553564514)
XLA Ops:
  7.2 0.7 all-gather.4.cloned.1.call-update
  8.0 0.7 all-gather.8.cloned.1.call-update
  8.7 0.7 all-gather.6.cloned.1.call-update
  9.5 0.6 add_reduce_fusion
  12.0 0.7 add_reduce_fusion.1
  15.9 0.8 fusion.88
  16.7 18.2 %all-gather.4.cloned.1.call-done = bf16[256,4096]{1,0:T(8,128)(2,1)} async-done(((bf16[64,4096]{1,0:T(8,128)(2,1)}), bf16[256,4096]{1,0:T(8,128)(2,1)}) %all-gather.4.cloned.1.call-update) | async-done | bytes 2097168 | tf_op jit(solution)/shard_map/all_gather | solution.py:121
  34.9 2.2 %fusion.53 = f32[256]{0:T(256)S(1)} fusion(bf16[256,4096]{1,0:T(8,128)(2,1)} %all-gather.4.cloned.1.call-done), kind=kLoop, calls=%fused_computation.78 | loop fusion | flops 3145472 | bytes 2098176 | tf_op jit(solution)/shard_map/reduce_sum | solution.py:29
  37.1 0.6 fusion.55
  37.8 0.6 copy-done.9
  38.4 0.7 convolution_convert_fusion.5
  39.1 1.6 copy-done.7
  40.7 1.0 convolution_convert_fusion.3
  41.7 1.5 collective-permute-start
  43.3 1.4 fusion.59
  44.7 0.7 convolution_convert_fusion.4
  45.4 0.7 collective-permute-done
  46.0 1.5 collective-permute-start.1
  47.5 33.3 %all_gather.16 = bf16[2048,128]{1,0:T(8,128)(2,1)S(1)} all-gather(bf16[256,128]{1,0:T(8,128)(2,1)S(1)} %convolution_convert_fusion.5), channel_id=1, replica_groups=mesh['sp'=8,'tp'=4] {'sp'}, dimensions={0}, use_global_device_ids=true | all-gather | bytes 589824 | tf_op jit(solution)/shard_map/all_gather | solution.py:135
  80.9 32.5 %all_gather.17 = bf16[2048,128]{1,0:T(8,128)(2,1)S(1)} all-gather(bf16[256,128]{1,0:T(8,128)(2,1)S(1)} %convolution_convert_fusion.4), channel_id=1, replica_groups=mesh['sp'=8,'tp'=4] {'sp'}, dimensions={0}, use_global_device_ids=true | all-gather | bytes 589824 | tf_op jit(solution)/shard_map/all_gather | solution.py:134
  113.3 1.0 copy.20
  114.3 0.1 copy.23
  114.5 15.4 %while.27 = (s32[]{:T(128)}, f32[128,1,2,128]{0,3,2,1:T(8,128)S(1)}, f32[128,1,2]{0,2,1:T(2,128)S(1)}, s32[]{:T(128)}, s32[]{:T(128)}, /*index=5*/bf16[2048,128]...) while((s32[]{:T(128)}, ...), condition=%wide.region_12.13_spmd.clone, body=%wide.region_8.12_spmd.clone.sunk | while | flops 175588480 | bytes 23864196 | solution.py:73
  114.6 0.2 broadcast_compare_fusion.5
  114.8 1.9 fusion.127
  116.6 2.5 %fusion.128 = f32[128,1,2,8,128]{0,3,2,1,4:T(8,128)S(1)} fusion(f32[128,1,2,8,128]{0,4,3,2,1:T(8,128)S(1)} %bitcast.178), kind=kOutput, calls=%fused_computation.56.clone.1 | output fusion | flops 33292288 | bytes 2097152 | tf_op jit(solution)/shard_map/reduce-window.2
  119.2 0.1 broadcast.117
  119.3 0.3 copy.37
  119.7 0.8 copy-done.2
  120.4 1.5 fusion.129
  121.9 0.2 fusion.130
  122.3 0.2 broadcast_compare_fusion.5
  122.5 1.8 fusion.127
  124.3 2.5 %fusion.128 = f32[128,1,2,8,128]{0,3,2,1,4:T(8,128)S(1)} fusion(f32[128,1,2,8,128]{0,4,3,2,1:T(8,128)S(1)} %bitcast.178), kind=kOutput, calls=%fused_computation.56.clone.1 | output fusion | flops 33292288 | bytes 2097152 | tf_op jit(solution)/shard_map/reduce-window.2
  126.9 0.1 broadcast.117
  127.0 0.3 copy.37
  127.3 0.8 copy-done.2
  128.1 1.5 fusion.129
  129.6 0.2 fusion.130
  129.9 0.1 collective-permute-start.3
  130.0 2.9 %fusion.58 = bf16[256,256]{1,0:T(8,128)(2,1)S(1)} fusion(f32[256,256]{1,0:T(8,128)} %fusion.59, bf16[256,4096]{1,0:T(8,128)(2,1)} %copy-done.1, bf16[4096,256]{1,0:T(8,128)(2,1)} %param.24), kind=kOutput, calls=%fused_computation.84 | convolution fusion | flops 537133056 | bytes 4587520 | tf_op jit(solution)/shard_map/dot_general | solution.py:115
  133.0 0.1 copy.21
  133.1 3.9 %collective-permute-start.6 = (bf16[2,256]{1,0:T(2,128)(2,1)S(1)}, bf16[2,256]{1,0:T(2,128)(2,1)S(1)}, u32[]{:S(2)}, u32[]{:S(2)}) collective-permute-start(bf16[2,256]{1,0:T(2,128)(2,1)S(1)} %slice.54), channel_id=1, source_target_pairs={{0,4},{4,8},{8,12},{12,16},{16,20},{20,24},{24,28},{1,5},{5,9},{9,... | collective-permute-start | bytes 3080 | tf_op jit(solution)/shard_map/ppermute | solution.py:24
  137.0 0.1 collective-permute-start.4
  137.1 7.9 %while.26 = (s32[]{:T(128)}, f32[128,1,2,128]{0,3,2,1:T(8,128)S(1)}, f32[128,1,2]{0,2,1:T(2,128)S(1)}, s32[]{:T(128)}, s32[]{:T(128)}, /*index=5*/bf16[2048,128]...) while((s32[]{:T(128)}, ...), condition=%wide.region_6.7_spmd.clone, body=%wide.region_2.6_spmd.clone.sunk | while | flops 175588480 | bytes 23864196 | solution.py:73
  137.4 0.2 broadcast_compare_fusion.4
  137.6 1.8 fusion.120
  139.4 2.5 %fusion.121 = f32[128,1,2,8,128]{0,3,2,1,4:T(8,128)S(1)} fusion(f32[128,1,2,8,128]{0,4,3,2,1:T(8,128)S(1)} %bitcast.179), kind=kOutput, calls=%fused_computation.20.clone.1 | output fusion | flops 33292288 | bytes 2097152 | tf_op jit(solution)/shard_map/reduce-window
  142.0 0.1 broadcast.116
  142.1 0.3 copy.35
  142.5 0.8 copy-done.3
  143.2 1.5 fusion.122
  144.7 0.2 fusion.123
  145.0 2.2 %collective-permute-start.5 = (bf16[128,256]{0,1:T(8,128)(2,1)}, bf16[128,256]{0,1:T(8,128)(2,1)S(1)}, u32[]{:S(2)}, u32[]{:S(2)}) collective-permute-start(bf16[128,256]{0,1:T(8,128)(2,1)} %collective-permute-done.4), channel_id=1, source_target_pairs={{0,16},{16,0},{4,20},{20,4},{8,24},{24,8},{12,28},{28,12},{1,17},{... | collective-permute-start | bytes 196616 | tf_op jit(solution)/shard_map/ppermute | solution.py:18
  147.2 6.6 %fusion.63 = f32[256,4096]{1,0:T(8,128)} fusion(bf16[4096,256]{1,0:T(8,128)(2,1)} %all-gather.8.cloned.1.call-done, bf16[256,4096]{1,0:T(8,128)(2,1)} %copy-done.1, bf16[4096,256]{1,0:T(8,128)(2,1)S(1)} %copy-done, bf16[256,256]{1,0:T(8,128)(2,1)} %copy-done.11, bf16[2,256]{1,0:T(2,128)(2,1)S(1)} %collective-permute-done.6, f32[256]{0:T(256)S(1)} %bitcast.186, ...), kind=kOutput, calls=%fused_computation.92 | convolution fusion | flops 1074921472 | bytes 10620928 | tf_op jit(solution)/shard_map/dot_general | solution.py:167
  153.9 5.0 %fusion.52 = bf16[256,4096]{1,0:T(8,128)(2,1)} fusion(f32[256,4096]{1,0:T(8,128)} %fusion.63, bf16[4096,256]{1,0:T(8,128)(2,1)} %all-gather.6.cloned.1.call-done, bf16[128,256]{0,1:T(8,128)(2,1)S(1)} %collective-permute-done.5, bf16[128,256]{0,1:T(8,128)(2,1)S(1)} %bitcast.180), kind=kOutput, calls=%fused_computation.77 | convolution fusion | flops 539230208 | bytes 8519680 | tf_op jit(solution)/shard_map/dot_general | solution.py:166
  158.9 1.3 collective-permute-start.7
  160.1 2.4 %collective-permute-done.7 = bf16[128,2]{0,1:T(2,128)(2,1)S(1)} collective-permute-done((bf16[128,2]{0,1:T(2,128)(2,1)S(1)}, bf16[128,2]{0,1:T(2,128)(2,1)S(1)}, u32[]{:S(2)}, u32[]{:S(2)}) %collective-permute-start.7) | collective-permute-done | bytes 544 | tf_op jit(solution)/shard_map/ppermute | solution.py:18
  162.5 1.2 collective-permute-start.8
  163.7 2.4 %collective-permute-done.8 = bf16[128,2]{0,1:T(2,128)(2,1)S(1)} collective-permute-done((bf16[128,2]{0,1:T(2,128)(2,1)S(1)}, bf16[128,2]{0,1:T(2,128)(2,1)S(1)}, u32[]{:S(2)}, u32[]{:S(2)}) %collective-permute-start.8) | collective-permute-done | bytes 544 | tf_op jit(solution)/shard_map/ppermute | solution.py:18
  166.1 0.8 collective-permute-start.9
  166.9 3.6 %collective-permute-done.9 = bf16[128,2]{0,1:T(2,128)(2,1)S(1)} collective-permute-done((bf16[128,2]{0,1:T(2,128)(2,1)S(1)}, bf16[128,2]{0,1:T(2,128)(2,1)S(1)}, u32[]{:S(2)}, u32[]{:S(2)}) %collective-permute-start.9) | collective-permute-done | bytes 544 | tf_op jit(solution)/shard_map/ppermute | solution.py:18
  170.5 0.6 fusion.84
  171.1 17.7 %reduce-scatter.2.cloned.1.call-done = bf16[64,4096]{1,0:T(8,128)(2,1)} async-done(((bf16[256,4096]{1,0:T(8,128)(2,1)}), bf16[64,4096]{1,0:T(8,128)(2,1)}) %reduce-scatter.2.cloned.1.call-update) | async-done | bytes 524304 | tf_op jit(solution)/shard_map/reduce_scatter | solution.py:171
  (94 shorter events, 0.6 us)
Async XLA Ops:
  7.2 140.1 %copy-start = (bf16[4096,256]{1,0:T(8,128)(2,1)S(1)}, bf16[4096,256]{1,0:T(8,128)(2,1)}, u32[]{:S(2)}) copy-start(bf16[4096,256]{1,0:T(8,128)(2,1)} %param.22) | copy-start | bytes 6291460
  7.2 29.9 %copy-start.20 = (f32[4096]{0:T(1024)S(1)}, f32[4096]{0:T(1024)}, u32[]{:S(2)}) copy-start(f32[4096]{0:T(1024)} %param.17) | copy-start | bytes 49156
  7.2 27.7 %all-gather.4.cloned.1.call-start = ((), (), s32[]{:S(2)}) async-start(), calls=%async_computation.1 | async-start | bytes 2621440 | tf_op jit(solution)/shard_map/all_gather | solution.py:121
  7.9 139.3 %all-gather.8.cloned.1.call-start = ((), (), s32[]{:S(2)}) async-start(), calls=%async_computation.3 | async-start | bytes 2359296 | tf_op jit(solution)/shard_map/all_gather | solution.py:165
  8.7 145.2 %all-gather.6.cloned.1.call-start = ((), (), s32[]{:S(2)}) async-start(), calls=%async_computation.2 | async-start | bytes 2359296 | tf_op jit(solution)/shard_map/all_gather | solution.py:165
  9.4 179.5 %reduce-scatter.2.cloned.1.call-start = ((), (), s32[]{:S(2)}) async-start(), calls=%async_computation.4 | async-start | bytes 2621440 | tf_op jit(solution)/shard_map/reduce_scatter | solution.py:171
  34.9 2.3 %copy-start.6 = (bf16[256,4096]{1,0:T(8,128)(2,1)S(1)}, bf16[256,4096]{1,0:T(8,128)(2,1)}, u32[]{:S(2)}) copy-start(bf16[256,4096]{1,0:T(8,128)(2,1)} %all-gather.4.cloned.1.call-done) | copy-start | bytes 6291460
  37.1 1.2 copy-start.9
  38.4 6.3 %copy-start.1 = (bf16[256,4096]{1,0:T(8,128)(2,1)}, bf16[256,4096]{1,0:T(8,128)(2,1)S(1)}, u32[]{:S(2)}) copy-start(bf16[256,4096]{1,0:T(8,128)(2,1)S(1)} %fusion.55) | copy-start | bytes 6291460
  38.4 2.3 %copy-start.7 = (bf16[4096,256]{1,0:T(8,128)(2,1)S(1)}, bf16[4096,256]{1,0:T(8,128)(2,1)}, u32[]{:S(2)}) copy-start(bf16[4096,256]{1,0:T(8,128)(2,1)} %param.18) | copy-start | bytes 6291460
  40.7 2.5 %copy-start.8 = (bf16[4096,256]{1,0:T(8,128)(2,1)S(1)}, bf16[4096,256]{1,0:T(8,128)(2,1)}, u32[]{:S(2)}) copy-start(bf16[4096,256]{1,0:T(8,128)(2,1)} %param.23) | copy-start | bytes 6291460
  41.7 3.0 %copy-start.10 = (bf16[4096,128]{1,0:T(8,128)(2,1)S(1)}, bf16[4096,128]{1,0:T(8,128)(2,1)}, u32[]{:S(2)}) copy-start(bf16[4096,128]{1,0:T(8,128)(2,1)} %param.19) | copy-start | bytes 3145732
  41.7 4.3 %collective-permute-start = (bf16[128,256]{0,1:T(8,128)(2,1)S(1)}, bf16[128,256]{0,1:T(8,128)(2,1)S(1)}, u32[]{:S(2)}, u32[]{:S(2)}) collective-permute-start(bf16[128,256]{0,1:T(8,128)(2,1)S(1)} %get-tuple-element.233), channel_id=1, source_target_pairs={{0,4},{4,0},{8,12},{12,8},{16,20},{20,16},{24,28},{28,24},{1,5},{5... | collective-permute-start | bytes 196616 | tf_op jit(solution)/shard_map/ppermute | solution.py:18
  44.7 69.8 %copy-start.21 = (f32[2]{0:T(128)S(1)}, f32[2]{0:T(128)}, u32[]{:S(2)}) copy-start(f32[2]{0:T(128)} %param.21) | copy-start | bytes 28
  46.0 34.8 %collective-permute-start.1 = (bf16[128,256]{0,1:T(8,128)(2,1)S(1)}, bf16[128,256]{0,1:T(8,128)(2,1)S(1)}, u32[]{:S(2)}, u32[]{:S(2)}) collective-permute-start(bf16[128,256]{0,1:T(8,128)(2,1)S(1)} %collective-permute-done), channel_id=1, source_target_pairs={{0,8},{8,0},{4,12},{12,4},{16,24},{24,16},{20,28},{28,20},{1,9},{9... | collective-permute-start | bytes 196616 | tf_op jit(solution)/shard_map/ppermute | solution.py:18
  80.9 33.5 %collective-permute-start.2 = (bf16[128,256]{0,1:T(8,128)(2,1)S(1)}, bf16[128,256]{0,1:T(8,128)(2,1)S(1)}, u32[]{:S(2)}, u32[]{:S(2)}) collective-permute-start(bf16[128,256]{0,1:T(8,128)(2,1)S(1)} %collective-permute-done.1), channel_id=1, source_target_pairs={{0,16},{16,0},{4,20},{20,4},{8,24},{24,8},{12,28},{28,12},{1,17},{... | collective-permute-start | bytes 196616 | tf_op jit(solution)/shard_map/ppermute | solution.py:18
  114.5 2.1 %copy-start.12 = (bf16[2048,128]{1,0:T(8,128)(2,1)}, bf16[2048,128]{1,0:T(8,128)(2,1)S(1)}, u32[]{:S(2)}) copy-start(bf16[2048,128]{1,0:T(8,128)(2,1)S(1)} %get-tuple-element.417) | copy-start | bytes 1572868 | tf_op jit(solution)/shard_map/while
  114.5 2.1 %copy-start.18 = (bf16[128,1,2,128]{3,0,2,1:T(8,128)(2,1)}, bf16[128,1,2,128]{3,0,2,1:T(8,128)(2,1)S(1)}, u32[]{:S(2)}) copy-start(bf16[128,1,2,128]{3,0,2,1:T(8,128)(2,1)S(1)} %get-tuple-element.418) | copy-start | bytes 196612 | tf_op jit(solution)/shard_map/while
  119.2 1.2 copy-start.2
  119.6 2.3 %copy-start.4 = (bf16[2048,128]{0,1:T(8,128)(2,1)S(1)}, bf16[2048,128]{0,1:T(8,128)(2,1)}, u32[]{:S(2)}) copy-start(bf16[2048,128]{0,1:T(8,128)(2,1)} %get-tuple-element.416) | copy-start | bytes 1572868 | tf_op jit(solution)/shard_map/while
  120.4 1.7 copy-start.13
  120.4 1.8 copy-start.19
  122.2 2.1 %copy-start.12 = (bf16[2048,128]{1,0:T(8,128)(2,1)}, bf16[2048,128]{1,0:T(8,128)(2,1)S(1)}, u32[]{:S(2)}) copy-start(bf16[2048,128]{1,0:T(8,128)(2,1)S(1)} %get-tuple-element.417) | copy-start | bytes 1572868 | tf_op jit(solution)/shard_map/while
  122.2 2.1 %copy-start.18 = (bf16[128,1,2,128]{3,0,2,1:T(8,128)(2,1)}, bf16[128,1,2,128]{3,0,2,1:T(8,128)(2,1)S(1)}, u32[]{:S(2)}) copy-start(bf16[128,1,2,128]{3,0,2,1:T(8,128)(2,1)S(1)} %get-tuple-element.418) | copy-start | bytes 196612 | tf_op jit(solution)/shard_map/while
  126.9 1.2 copy-start.2
  127.3 2.3 %copy-start.4 = (bf16[2048,128]{0,1:T(8,128)(2,1)S(1)}, bf16[2048,128]{0,1:T(8,128)(2,1)}, u32[]{:S(2)}) copy-start(bf16[2048,128]{0,1:T(8,128)(2,1)} %get-tuple-element.416) | copy-start | bytes 1572868 | tf_op jit(solution)/shard_map/while
  128.1 1.7 copy-start.13
  128.1 1.8 copy-start.19
  129.9 7.1 %collective-permute-start.3 = (bf16[128,256]{0,1:T(8,128)(2,1)S(1)}, bf16[128,256]{0,1:T(8,128)(2,1)}, u32[]{:S(2)}, u32[]{:S(2)}) collective-permute-start(bf16[128,256]{0,1:T(8,128)(2,1)S(1)} %bitcast.182), channel_id=1, source_target_pairs={{0,4},{4,0},{8,12},{12,8},{16,20},{20,16},{24,28},{28,24},{1,5},{5... | collective-permute-start | bytes 196616 | tf_op jit(solution)/shard_map/ppermute | solution.py:18
  133.0 4.2 %copy-start.11 = (bf16[256,256]{1,0:T(8,128)(2,1)}, bf16[256,256]{1,0:T(8,128)(2,1)S(1)}, u32[]{:S(2)}) copy-start(bf16[256,256]{1,0:T(8,128)(2,1)S(1)} %fusion.58) | copy-start | bytes 393220
  133.1 14.1 %collective-permute-start.6 = (bf16[2,256]{1,0:T(2,128)(2,1)S(1)}, bf16[2,256]{1,0:T(2,128)(2,1)S(1)}, u32[]{:S(2)}, u32[]{:S(2)}) collective-permute-start(bf16[2,256]{1,0:T(2,128)(2,1)S(1)} %slice.54), channel_id=1, source_target_pairs={{0,4},{4,8},{8,12},{12,16},{16,20},{20,24},{24,28},{1,5},{5,9},{9,... | collective-permute-start | bytes 3080 | tf_op jit(solution)/shard_map/ppermute | solution.py:24
  137.0 8.0 %collective-permute-start.4 = (bf16[128,256]{0,1:T(8,128)(2,1)}, bf16[128,256]{0,1:T(8,128)(2,1)}, u32[]{:S(2)}, u32[]{:S(2)}) collective-permute-start(bf16[128,256]{0,1:T(8,128)(2,1)} %collective-permute-done.3), channel_id=1, source_target_pairs={{0,8},{8,0},{4,12},{12,4},{16,24},{24,16},{20,28},{28,20},{1,9},{9... | collective-permute-start | bytes 196616 | tf_op jit(solution)/shard_map/ppermute | solution.py:18
  137.3 2.1 %copy-start.14 = (bf16[2048,128]{1,0:T(8,128)(2,1)}, bf16[2048,128]{1,0:T(8,128)(2,1)S(1)}, u32[]{:S(2)}) copy-start(bf16[2048,128]{1,0:T(8,128)(2,1)S(1)} %get-tuple-element.462) | copy-start | bytes 1572868 | tf_op jit(solution)/shard_map/while
  137.4 2.1 %copy-start.16 = (bf16[128,1,2,128]{3,0,2,1:T(8,128)(2,1)}, bf16[128,1,2,128]{3,0,2,1:T(8,128)(2,1)S(1)}, u32[]{:S(2)}) copy-start(bf16[128,1,2,128]{3,0,2,1:T(8,128)(2,1)S(1)} %get-tuple-element.463) | copy-start | bytes 196612 | tf_op jit(solution)/shard_map/while
  142.0 1.2 copy-start.3
  142.5 2.3 %copy-start.5 = (bf16[2048,128]{0,1:T(8,128)(2,1)S(1)}, bf16[2048,128]{0,1:T(8,128)(2,1)}, u32[]{:S(2)}) copy-start(bf16[2048,128]{0,1:T(8,128)(2,1)} %get-tuple-element.461) | copy-start | bytes 1572868 | tf_op jit(solution)/shard_map/while
  143.2 1.7 copy-start.15
  143.2 1.8 copy-start.17
  145.0 8.8 %collective-permute-start.5 = (bf16[128,256]{0,1:T(8,128)(2,1)}, bf16[128,256]{0,1:T(8,128)(2,1)S(1)}, u32[]{:S(2)}, u32[]{:S(2)}) collective-permute-start(bf16[128,256]{0,1:T(8,128)(2,1)} %collective-permute-done.4), channel_id=1, source_target_pairs={{0,16},{16,0},{4,20},{20,4},{8,24},{24,8},{12,28},{28,12},{1,17},{... | collective-permute-start | bytes 196616 | tf_op jit(solution)/shard_map/ppermute | solution.py:18
  158.9 3.6 %collective-permute-start.7 = (bf16[128,2]{0,1:T(2,128)(2,1)S(1)}, bf16[128,2]{0,1:T(2,128)(2,1)S(1)}, u32[]{:S(2)}, u32[]{:S(2)}) collective-permute-start(bf16[128,2]{0,1:T(2,128)(2,1)S(1)} %convert_bitcast_fusion), channel_id=1, source_target_pairs={{0,4},{4,0},{8,12},{12,8},{16,20},{20,16},{24,28},{28,24},{1,5},{5... | collective-permute-start | bytes 1544 | tf_op jit(solution)/shard_map/ppermute | solution.py:18
  162.5 3.6 %collective-permute-start.8 = (bf16[128,2]{0,1:T(2,128)(2,1)S(1)}, bf16[128,2]{0,1:T(2,128)(2,1)S(1)}, u32[]{:S(2)}, u32[]{:S(2)}) collective-permute-start(bf16[128,2]{0,1:T(2,128)(2,1)S(1)} %collective-permute-done.7), channel_id=1, source_target_pairs={{0,8},{8,0},{4,12},{12,4},{16,24},{24,16},{20,28},{28,20},{1,9},{9... | collective-permute-start | bytes 1544 | tf_op jit(solution)/shard_map/ppermute | solution.py:18
  166.1 4.5 %collective-permute-start.9 = (bf16[128,2]{0,1:T(2,128)(2,1)S(1)}, bf16[128,2]{0,1:T(2,128)(2,1)S(1)}, u32[]{:S(2)}, u32[]{:S(2)}) collective-permute-start(bf16[128,2]{0,1:T(2,128)(2,1)S(1)} %collective-permute-done.8), channel_id=1, source_target_pairs={{0,16},{16,0},{4,20},{20,4},{8,24},{24,8},{12,28},{28,12},{1,17},{... | collective-permute-start | bytes 1544 | tf_op jit(solution)/shard_map/ppermute | solution.py:18
Sparse Core Ops, SparseCore 0:
  9.6 25.2 all-gather.3
  37.0 56.6 all-gather.7
  95.9 49.0 all-gather.5
  159.0 29.8 reduce-scatter.1
where the time goes:
time: 196 us; the launch traced here: 195 us
  blocking collectives  65.8 us (34%)
  waiting for transfers between devices  47 us (24%)
  matrix products  24.6 us (13%)
  between operations  19.2 us (10%)
  other arithmetic  17.5 us (9%)
  starting transfers between devices  12.7 us (6%)
  local copies, waits for them, and re-layouts  7.99 us (4%)
    all_gather x1, blocking collectives, local(): lax.all_gather(values, 'sp', axis=0, tiled=True)  33.3 us
    all_gather x1, blocking collectives, local(): lax.all_gather(keys, 'sp', axis=0, tiled=True)  32.5 us
    all_gather x1, waiting for transfers between devices, local(): projected = project(lax.all_gather(tokens, 'tp', axis=0, tiled=True))  18.2 us
    reduce_scatter x1, waiting for transfers between devices, local(): lax.psum_scatter(rounded.astype(jnp.bfloat16), 'tp', scatter_dimension=0,...  17.7 us
    ppermute x9, waiting for transfers between devices, swapped(): return lax.ppermute(block, axis, route)  9.08 us
    ppermute x9, starting transfers between devices, swapped(): return lax.ppermute(block, axis, route)  8.63 us
    another operation x7, other arithmetic  7.65 us
    dot_general x5, matrix products, project(): jnp.dot(normed, weight, preferred_element_type=jnp.float32)  6.7 us
  transfers between devices with their start and end apart: 14, of which 6 were waited for; matrix products, arithmetic and copies ran while one was open for 21% of the time, Pallas kernels for 0%

commit v1 on v0

--- a/solution.py
+++ b/solution.py
@@ -131,7 +131,15 @@
     products = (gate_c.astype(jnp.float32) * inputs_u.astype(jnp.float32)).astype(jnp.bfloat16)
     previous = shifted(products[tok_count - (CONV_K - 1) :], "sp", 1)
     key_whole, value_whole = (
-        lax.all_gather(keys, "sp", axis=0, tiled=True),
+        jnp.concatenate(
+            lax.all_to_all(
+                jnp.stack([keys for _ in range(lax.axis_size("sp"))], axis=0),
+                axis_name="sp",
+                split_axis=0,
+                concat_axis=0,
+            ),
+            axis=0,
+        ),
         lax.all_gather(values, "sp", axis=0, tiled=True),
     )
     local_heads = queries.shape[1] // HEAD_DIM

time: 196 us -> 193 us (0.985)
  blocking collectives: 65.8 us -> 33.2 us
  waiting for transfers between devices: 47 us -> 65.8 us
  starting transfers between devices: 12.7 us -> 22.3 us
  matrix products: 24.6 us -> 26.8 us
    all_gather x1 -> x0, blocking collectives: 32.5 us -> none  [local(): lax.all_gather(keys, 'sp', axis=0, tiled=True)]
    all_gather x2, waiting for transfers between devices: 0.01 us -> 10.8 us  [local(): pieces = lax.all_gather((w_out_att, w_out_conv), 'sp', axis=0, tiled=True)]
    ppermute x9, waiting for transfers between devices: 9.08 us -> 15.9 us  [swapped(): return lax.ppermute(block, axis, route)]
    all_to_all x0 -> x1, starting transfers between devices: none -> 5.52 us  [local(): lax.all_to_all(jnp.stack([keys for _ in range(lax.axis_size('sp'))], axis...]
    ppermute x9, starting transfers between devices: 8.63 us -> 12.6 us  [swapped(): return lax.ppermute(block, axis, route)]
    dot_general x5, matrix products: 6.7 us -> 9.07 us  [project(): jnp.dot(normed, weight, preferred_element_type=jnp.float32)]
  transfers between devices with their start and end apart: 14 -> 15, of which waited for: 6 -> 9; matrix products, arithmetic and copies ran while one was open for 21% -> 23% of each run, Pallas kernels for 0% -> 0%
where the time goes in v1:
time: 193 us
  waiting for transfers between devices  65.8 us (34%)
  blocking collectives  33.2 us (17%)
  matrix products  26.8 us (14%)
  starting transfers between devices  22.3 us (12%)
  between operations  18.9 us (10%)
  other arithmetic  17.5 us (9%)
  local copies, waits for them, and re-layouts  8.05 us (4%)
    all_gather x1, blocking collectives, local(): lax.all_gather(values, 'sp', axis=0, tiled=True)  33.2 us
    all_gather x1, waiting for transfers between devices, local(): projected = project(lax.all_gather(tokens, 'tp', axis=0, tiled=True))  19.1 us
    reduce_scatter x1, waiting for transfers between devices, local(): lax.psum_scatter(rounded.astype(jnp.bfloat16), 'tp', scatter_dimension=0,...  17.6 us
    ppermute x9, waiting for transfers between devices, swapped(): return lax.ppermute(block, axis, route)  15.9 us
    ppermute x9, starting transfers between devices, swapped(): return lax.ppermute(block, axis, route)  12.6 us
    all_gather x2, waiting for transfers between devices, local(): pieces = lax.all_gather((w_out_att, w_out_conv), 'sp', axis=0, tiled=True)  10.8 us
    dot_general x5, matrix products, project(): jnp.dot(normed, weight, preferred_element_type=jnp.float32)  9.07 us
    another operation x7, other arithmetic  7.65 us
  transfers between devices with their start and end apart: 15, of which 9 were waited for; matrix products, arithmetic and copies ran while one was open for 23% of the time, Pallas kernels for 0%

profile of v1, /device:TPU:0, one launch (start us, length us, event | category | flops | bytes accessed | tf_op | source)
XLA Modules:
  0.0 193.0 jit_solution(14824080870777596703)
XLA Ops:
  7.2 0.7 all-gather.4.cloned.1.call-update
  8.0 0.7 all-gather.8.cloned.1.call-update
  8.7 0.7 all-gather.6.cloned.1.call-update
  9.4 0.6 add_reduce_fusion
  12.0 0.6 add_reduce_fusion.1
  15.0 0.8 fusion.88
  15.8 19.1 %all-gather.4.cloned.1.call-done = bf16[256,4096]{1,0:T(8,128)(2,1)} async-done(((bf16[64,4096]{1,0:T(8,128)(2,1)}), bf16[256,4096]{1,0:T(8,128)(2,1)}) %all-gather.4.cloned.1.call-update) | async-done | bytes 2097168 | tf_op jit(solution)/shard_map/all_gather | solution.py:121
  34.9 2.2 %fusion.53 = f32[256]{0:T(256)S(1)} fusion(bf16[256,4096]{1,0:T(8,128)(2,1)} %all-gather.4.cloned.1.call-done), kind=kLoop, calls=%fused_computation.78 | loop fusion | flops 3145472 | bytes 2098176 | tf_op jit(solution)/shard_map/reduce_sum | solution.py:29
  37.1 0.6 fusion.55
  37.8 1.4 copy-done.1
  39.2 0.7 convolution_convert_fusion.4
  39.9 0.9 stack.2
  40.8 5.5 %all-to-all-start = ((bf16[8,256,128]{2,1,0:T(8,128)(2,1)}), bf16[8,256,128]{2,1,0:T(8,128)(2,1)S(1)}, u32[]{:S(2)}, u32[]{:S(2)}) async-start(bf16[8,256,128]{2,1,0:T(8,128)(2,1)} %stack.2), calls=%async_computation | async-start | bytes 1048576 | tf_op jit(solution)/shard_map/all_to_all | solution.py:135
  46.3 3.3 %convolution_convert_fusion.3 = bf16[256,256]{0,1:T(8,128)(2,1)S(1)} fusion(bf16[256,4096]{1,0:T(8,128)(2,1)} %copy-done.1, bf16[4096,256]{1,0:T(8,128)(2,1)} %param.18), kind=kOutput, calls=%fused_computation.91 | convolution fusion | flops 536936448 | bytes 4325376 | tf_op jit(solution)/shard_map/dot_general | solution.py:115
  49.7 2.0 %collective-permute-start = (bf16[128,256]{0,1:T(8,128)(2,1)S(1)}, bf16[128,256]{0,1:T(8,128)(2,1)S(1)}, u32[]{:S(2)}, u32[]{:S(2)}) collective-permute-start(bf16[128,256]{0,1:T(8,128)(2,1)S(1)} %get-tuple-element.233), channel_id=1, source_target_pairs={{0,4},{4,0},{8,12},{12,8},{16,20},{20,16},{24,28},{28,24},{1,5},{5... | collective-permute-start | bytes 196616 | tf_op jit(solution)/shard_map/ppermute | solution.py:18
  51.7 1.4 fusion.59
  53.1 1.2 collective-permute-done
  54.4 1.8 collective-permute-start.1
  56.2 0.7 convolution_convert_fusion.5
  56.9 7.0 %collective-permute-done.1 = bf16[128,256]{0,1:T(8,128)(2,1)S(1)} collective-permute-done((bf16[128,256]{0,1:T(8,128)(2,1)S(1)}, bf16[128,256]{0,1:T(8,128)(2,1)S(1)}, u32[]{:S(2)}, u32[]{:S(2)}) %collective-permute-start.1) | collective-permute-done | bytes 65568 | tf_op jit(solution)/shard_map/ppermute | solution.py:18
  63.9 4.6 %collective-permute-start.2 = (bf16[128,256]{0,1:T(8,128)(2,1)S(1)}, bf16[128,256]{0,1:T(8,128)(2,1)S(1)}, u32[]{:S(2)}, u32[]{:S(2)}) collective-permute-start(bf16[128,256]{0,1:T(8,128)(2,1)S(1)} %collective-permute-done.1), channel_id=1, source_target_pairs={{0,16},{16,0},{4,20},{20,4},{8,24},{24,8},{12,28},{28,12},{1,17},{... | collective-permute-start | bytes 196616 | tf_op jit(solution)/shard_map/ppermute | solution.py:18
  68.5 33.2 %all_gather.13 = bf16[2048,128]{1,0:T(8,128)(2,1)S(1)} all-gather(bf16[256,128]{1,0:T(8,128)(2,1)S(1)} %convolution_convert_fusion.5), channel_id=1, replica_groups=mesh['sp'=8,'tp'=4] {'sp'}, dimensions={0}, use_global_device_ids=true | all-gather | bytes 589824 | tf_op jit(solution)/shard_map/all_gather | solution.py:143
  101.7 1.0 copy.20
  102.7 0.1 copy.23
  102.9 15.4 %while.27 = (s32[]{:T(128)}, f32[128,1,2,128]{0,3,2,1:T(8,128)S(1)}, f32[128,1,2]{0,2,1:T(2,128)S(1)}, s32[]{:T(128)}, s32[]{:T(128)}, /*index=5*/bf16[2048,128]...) while((s32[]{:T(128)}, ...), condition=%wide.region_12.13_spmd.clone, body=%wide.region_8.12_spmd.clone.sunk | while | flops 175588480 | bytes 23864196 | solution.py:73
  102.9 0.2 broadcast_compare_fusion.5
  103.1 1.8 fusion.127
  105.0 2.5 %fusion.128 = f32[128,1,2,8,128]{0,3,2,1,4:T(8,128)S(1)} fusion(f32[128,1,2,8,128]{0,4,3,2,1:T(8,128)S(1)} %bitcast.179), kind=kOutput, calls=%fused_computation.56.clone.1 | output fusion | flops 33292288 | bytes 2097152 | tf_op jit(solution)/shard_map/reduce-window.2
  107.6 0.3 copy.37
  108.0 0.8 copy-done.3
  108.8 1.5 fusion.129
  110.3 0.2 fusion.130
  110.6 0.2 broadcast_compare_fusion.5
  110.8 1.8 fusion.127
  112.7 2.5 %fusion.128 = f32[128,1,2,8,128]{0,3,2,1,4:T(8,128)S(1)} fusion(f32[128,1,2,8,128]{0,4,3,2,1:T(8,128)S(1)} %bitcast.179), kind=kOutput, calls=%fused_computation.56.clone.1 | output fusion | flops 33292288 | bytes 2097152 | tf_op jit(solution)/shard_map/reduce-window.2
  115.3 0.3 copy.37
  115.7 0.8 copy-done.3
  116.5 1.5 fusion.129
  118.0 0.2 fusion.130
  118.3 0.1 collective-permute-start.3
  118.3 3.0 %fusion.58 = bf16[256,256]{1,0:T(8,128)(2,1)S(1)} fusion(f32[256,256]{1,0:T(8,128)} %fusion.59, bf16[256,4096]{1,0:T(8,128)(2,1)} %copy-done.1, bf16[4096,256]{1,0:T(8,128)(2,1)} %param.24), kind=kOutput, calls=%fused_computation.84 | convolution fusion | flops 537133056 | bytes 4587520 | tf_op jit(solution)/shard_map/dot_general | solution.py:115
  121.3 4.1 %collective-permute-start.6 = (bf16[2,256]{1,0:T(2,128)(2,1)S(1)}, bf16[2,256]{1,0:T(2,128)(2,1)S(1)}, u32[]{:S(2)}, u32[]{:S(2)}) collective-permute-start(bf16[2,256]{1,0:T(2,128)(2,1)S(1)} %slice.54), channel_id=1, source_target_pairs={{0,4},{4,8},{8,12},{12,16},{16,20},{20,24},{24,28},{1,5},{5,9},{9,... | collective-permute-start | bytes 3080 | tf_op jit(solution)/shard_map/ppermute | solution.py:24
  126.0 0.1 copy.21
  126.1 0.1 collective-permute-start.4
  126.2 0.3 collective-permute-done.6
  126.5 6.5 %fusion.63 = f32[256,4096]{1,0:T(8,128)} fusion(bf16[4096,256]{1,0:T(8,128)(2,1)} %all-gather.8.cloned.1.call-done, bf16[256,4096]{1,0:T(8,128)(2,1)} %copy-done.1, bf16[4096,256]{1,0:T(8,128)(2,1)S(1)} %copy-done, bf16[256,256]{1,0:T(8,128)(2,1)S(1)} %fusion.58, bf16[2,256]{1,0:T(2,128)(2,1)S(1)} %collective-permute-done.6, f32[256]{0:T(256)S(1)} %bitcast.188, ...), kind=kOutput, calls=%fused_computation.92 | convolution fusion | flops 1074921472 | bytes 10620928 | tf_op jit(solution)/shard_map/dot_general | solution.py:175
  133.1 7.7 %while.26 = (s32[]{:T(128)}, f32[128,1,2,128]{0,3,2,1:T(8,128)S(1)}, f32[128,1,2]{0,2,1:T(2,128)S(1)}, s32[]{:T(128)}, s32[]{:T(128)}, /*index=5*/bf16[2048,128]...) while((s32[]{:T(128)}, ...), condition=%wide.region_6.7_spmd.clone, body=%wide.region_2.6_spmd.clone.sunk | while | flops 175588480 | bytes 23864196 | solution.py:73
  133.1 0.2 broadcast_compare_fusion.4
  133.4 1.8 fusion.120
  135.2 2.5 %fusion.121 = f32[128,1,2,8,128]{0,3,2,1,4:T(8,128)S(1)} fusion(f32[128,1,2,8,128]{0,4,3,2,1:T(8,128)S(1)} %bitcast.180), kind=kOutput, calls=%fused_computation.20.clone.1 | output fusion | flops 33292288 | bytes 2097152 | tf_op jit(solution)/shard_map/reduce-window
  137.8 0.3 copy.35
  138.2 0.8 copy-done.4
  139.0 1.5 fusion.122
  140.5 0.2 fusion.123
  140.8 10.8 %all-gather.6.cloned.1.call-done = bf16[4096,256]{1,0:T(8,128)(2,1)} async-done(((bf16[512,256]{1,0:T(8,128)(2,1)}), bf16[4096,256]{1,0:T(8,128)(2,1)}) %all-gather.6.cloned.1.call-update) | async-done | bytes 2097168 | tf_op jit(solution)/shard_map/all_gather | solution.py:173
  151.6 5.0 %fusion.52 = bf16[256,4096]{1,0:T(8,128)(2,1)} fusion(f32[256,4096]{1,0:T(8,128)} %fusion.63, bf16[4096,256]{1,0:T(8,128)(2,1)} %all-gather.6.cloned.1.call-done, bf16[128,256]{0,1:T(8,128)(2,1)S(1)} %collective-permute-done.5, bf16[128,256]{0,1:T(8,128)(2,1)S(1)} %bitcast.182), kind=kOutput, calls=%fused_computation.77 | convolution fusion | flops 539230208 | bytes 8519680 | tf_op jit(solution)/shard_map/dot_general | solution.py:174
  156.6 0.6 collective-permute-start.7
  157.3 3.0 %collective-permute-done.7 = bf16[128,2]{0,1:T(2,128)(2,1)S(1)} collective-permute-done((bf16[128,2]{0,1:T(2,128)(2,1)S(1)}, bf16[128,2]{0,1:T(2,128)(2,1)S(1)}, u32[]{:S(2)}, u32[]{:S(2)}) %collective-permute-start.7) | collective-permute-done | bytes 544 | tf_op jit(solution)/shard_map/ppermute | solution.py:18
  160.3 1.5 collective-permute-start.8
  161.8 2.0 %collective-permute-done.8 = bf16[128,2]{0,1:T(2,128)(2,1)S(1)} collective-permute-done((bf16[128,2]{0,1:T(2,128)(2,1)S(1)}, bf16[128,2]{0,1:T(2,128)(2,1)S(1)}, u32[]{:S(2)}, u32[]{:S(2)}) %collective-permute-start.8) | collective-permute-done | bytes 544 | tf_op jit(solution)/shard_map/ppermute | solution.py:18
  163.9 1.9 collective-permute-start.9
  165.7 2.6 %collective-permute-done.9 = bf16[128,2]{0,1:T(2,128)(2,1)S(1)} collective-permute-done((bf16[128,2]{0,1:T(2,128)(2,1)S(1)}, bf16[128,2]{0,1:T(2,128)(2,1)S(1)}, u32[]{:S(2)}, u32[]{:S(2)}) %collective-permute-start.9) | collective-permute-done | bytes 544 | tf_op jit(solution)/shard_map/ppermute | solution.py:18
  168.3 0.6 fusion.84
  168.9 17.6 %reduce-scatter.2.cloned.1.call-done = bf16[64,4096]{1,0:T(8,128)(2,1)} async-done(((bf16[256,4096]{1,0:T(8,128)(2,1)}), bf16[64,4096]{1,0:T(8,128)(2,1)}) %reduce-scatter.2.cloned.1.call-update) | async-done | bytes 524304 | tf_op jit(solution)/shard_map/reduce_scatter | solution.py:179
  (94 shorter events, 0.8 us)
Async XLA Ops:
  7.2 119.4 %copy-start = (bf16[4096,256]{1,0:T(8,128)(2,1)S(1)}, bf16[4096,256]{1,0:T(8,128)(2,1)}, u32[]{:S(2)}) copy-start(bf16[4096,256]{1,0:T(8,128)(2,1)} %param.22) | copy-start | bytes 6291460
  7.2 29.9 %copy-start.19 = (f32[4096]{0:T(1024)S(1)}, f32[4096]{0:T(1024)}, u32[]{:S(2)}) copy-start(f32[4096]{0:T(1024)} %param.17) | copy-start | bytes 49156
  7.2 27.7 %all-gather.4.cloned.1.call-start = ((), (), s32[]{:S(2)}) async-start(), calls=%async_computation.2 | async-start | bytes 2621440 | tf_op jit(solution)/shard_map/all_gather | solution.py:121
  7.9 118.6 %all-gather.8.cloned.1.call-start = ((), (), s32[]{:S(2)}) async-start(), calls=%async_computation.4 | async-start | bytes 2359296 | tf_op jit(solution)/shard_map/all_gather | solution.py:173
  8.7 143.0 %all-gather.6.cloned.1.call-start = ((), (), s32[]{:S(2)}) async-start(), calls=%async_computation.3 | async-start | bytes 2359296 | tf_op jit(solution)/shard_map/all_gather | solution.py:173
  34.9 2.3 %copy-start.7 = (bf16[256,4096]{1,0:T(8,128)(2,1)S(1)}, bf16[256,4096]{1,0:T(8,128)(2,1)}, u32[]{:S(2)}) copy-start(bf16[256,4096]{1,0:T(8,128)(2,1)} %all-gather.4.cloned.1.call-done) | copy-start | bytes 6291460
  37.1 2.1 %copy-start.9 = (bf16[4096,128]{1,0:T(8,128)(2,1)S(1)}, bf16[4096,128]{1,0:T(8,128)(2,1)}, u32[]{:S(2)}) copy-start(bf16[4096,128]{1,0:T(8,128)(2,1)} %param.19) | copy-start | bytes 3145732
  37.8 1.4 copy-start.1
  40.8 62.1 %all-to-all-start = ((bf16[8,256,128]{2,1,0:T(8,128)(2,1)}), bf16[8,256,128]{2,1,0:T(8,128)(2,1)S(1)}, u32[]{:S(2)}, u32[]{:S(2)}) async-start(bf16[8,256,128]{2,1,0:T(8,128)(2,1)} %stack.2), calls=%async_computation | async-start | bytes 1048576 | tf_op jit(solution)/shard_map/all_to_all | solution.py:135
  46.3 140.2 %reduce-scatter.2.cloned.1.call-start = ((), (), s32[]{:S(2)}) async-start(), calls=%async_computation.5 | async-start | bytes 2621440 | tf_op jit(solution)/shard_map/reduce_scatter | solution.py:179
  46.3 5.4 %copy-start.2 = (bf16[256,4096]{1,0:T(8,128)(2,1)S(1)}, bf16[256,4096]{1,0:T(8,128)(2,1)}, u32[]{:S(2)}) copy-start(bf16[256,4096]{1,0:T(8,128)(2,1)} %copy-done.1) | copy-start | bytes 6291460
  46.3 5.4 %copy-start.8 = (bf16[4096,256]{1,0:T(8,128)(2,1)S(1)}, bf16[4096,256]{1,0:T(8,128)(2,1)}, u32[]{:S(2)}) copy-start(bf16[4096,256]{1,0:T(8,128)(2,1)} %param.23) | copy-start | bytes 6291460
  49.7 6.5 %copy-start.10 = (bf16[4096,128]{1,0:T(8,128)(2,1)S(1)}, bf16[4096,128]{1,0:T(8,128)(2,1)}, u32[]{:S(2)}) copy-start(bf16[4096,128]{1,0:T(8,128)(2,1)} %param.20) | copy-start | bytes 3145732
  49.7 4.7 %collective-permute-start = (bf16[128,256]{0,1:T(8,128)(2,1)S(1)}, bf16[128,256]{0,1:T(8,128)(2,1)S(1)}, u32[]{:S(2)}, u32[]{:S(2)}) collective-permute-start(bf16[128,256]{0,1:T(8,128)(2,1)S(1)} %get-tuple-element.233), channel_id=1, source_target_pairs={{0,4},{4,0},{8,12},{12,8},{16,20},{20,16},{24,28},{28,24},{1,5},{5... | collective-permute-start | bytes 196616 | tf_op jit(solution)/shard_map/ppermute | solution.py:18
  53.1 49.7 %copy-start.20 = (f32[2]{0:T(128)S(1)}, f32[2]{0:T(128)}, u32[]{:S(2)}) copy-start(f32[2]{0:T(128)} %param.21) | copy-start | bytes 28
  54.4 9.6 %collective-permute-start.1 = (bf16[128,256]{0,1:T(8,128)(2,1)S(1)}, bf16[128,256]{0,1:T(8,128)(2,1)S(1)}, u32[]{:S(2)}, u32[]{:S(2)}) collective-permute-start(bf16[128,256]{0,1:T(8,128)(2,1)S(1)} %collective-permute-done), channel_id=1, source_target_pairs={{0,8},{8,0},{4,12},{12,4},{16,24},{24,16},{20,28},{28,20},{1,9},{9... | collective-permute-start | bytes 196616 | tf_op jit(solution)/shard_map/ppermute | solution.py:18
  63.9 38.8 %collective-permute-start.2 = (bf16[128,256]{0,1:T(8,128)(2,1)S(1)}, bf16[128,256]{0,1:T(8,128)(2,1)S(1)}, u32[]{:S(2)}, u32[]{:S(2)}) collective-permute-start(bf16[128,256]{0,1:T(8,128)(2,1)S(1)} %collective-permute-done.1), channel_id=1, source_target_pairs={{0,16},{16,0},{4,20},{20,4},{8,24},{24,8},{12,28},{28,12},{1,17},{... | collective-permute-start | bytes 196616 | tf_op jit(solution)/shard_map/ppermute | solution.py:18
  102.9 2.1 %copy-start.11 = (bf16[2048,128]{1,0:T(8,128)(2,1)}, bf16[2048,128]{1,0:T(8,128)(2,1)S(1)}, u32[]{:S(2)}) copy-start(bf16[2048,128]{1,0:T(8,128)(2,1)S(1)} %get-tuple-element.417) | copy-start | bytes 1572868 | tf_op jit(solution)/shard_map/while
  102.9 2.1 %copy-start.17 = (bf16[128,1,2,128]{3,0,2,1:T(8,128)(2,1)}, bf16[128,1,2,128]{3,0,2,1:T(8,128)(2,1)S(1)}, u32[]{:S(2)}) copy-start(bf16[128,1,2,128]{3,0,2,1:T(8,128)(2,1)S(1)} %get-tuple-element.418) | copy-start | bytes 196612 | tf_op jit(solution)/shard_map/while
  107.5 1.2 copy-start.3
  108.0 2.3 %copy-start.5 = (bf16[2048,128]{0,1:T(8,128)(2,1)S(1)}, bf16[2048,128]{0,1:T(8,128)(2,1)}, u32[]{:S(2)}) copy-start(bf16[2048,128]{0,1:T(8,128)(2,1)} %get-tuple-element.416) | copy-start | bytes 1572868 | tf_op jit(solution)/shard_map/while
  108.8 1.7 copy-start.12
  108.8 1.8 copy-start.18
  110.6 2.1 %copy-start.11 = (bf16[2048,128]{1,0:T(8,128)(2,1)}, bf16[2048,128]{1,0:T(8,128)(2,1)S(1)}, u32[]{:S(2)}) copy-start(bf16[2048,128]{1,0:T(8,128)(2,1)S(1)} %get-tuple-element.417) | copy-start | bytes 1572868 | tf_op jit(solution)/shard_map/while
  110.6 2.1 %copy-start.17 = (bf16[128,1,2,128]{3,0,2,1:T(8,128)(2,1)}, bf16[128,1,2,128]{3,0,2,1:T(8,128)(2,1)S(1)}, u32[]{:S(2)}) copy-start(bf16[128,1,2,128]{3,0,2,1:T(8,128)(2,1)S(1)} %get-tuple-element.418) | copy-start | bytes 196612 | tf_op jit(solution)/shard_map/while
  115.2 1.2 copy-start.3
  115.7 2.3 %copy-start.5 = (bf16[2048,128]{0,1:T(8,128)(2,1)S(1)}, bf16[2048,128]{0,1:T(8,128)(2,1)}, u32[]{:S(2)}) copy-start(bf16[2048,128]{0,1:T(8,128)(2,1)} %get-tuple-element.416) | copy-start | bytes 1572868 | tf_op jit(solution)/shard_map/while
  116.5 1.7 copy-start.12
  116.5 1.8 copy-start.18
  118.3 7.9 %collective-permute-start.3 = (bf16[128,256]{0,1:T(8,128)(2,1)S(1)}, bf16[128,256]{0,1:T(8,128)(2,1)S(1)}, u32[]{:S(2)}, u32[]{:S(2)}) collective-permute-start(bf16[128,256]{0,1:T(8,128)(2,1)S(1)} %bitcast.184), channel_id=1, source_target_pairs={{0,4},{4,0},{8,12},{12,8},{16,20},{20,16},{24,28},{28,24},{1,5},{5... | collective-permute-start | bytes 196616 | tf_op jit(solution)/shard_map/ppermute | solution.py:18
  121.3 5.2 %collective-permute-start.6 = (bf16[2,256]{1,0:T(2,128)(2,1)S(1)}, bf16[2,256]{1,0:T(2,128)(2,1)S(1)}, u32[]{:S(2)}, u32[]{:S(2)}) collective-permute-start(bf16[2,256]{1,0:T(2,128)(2,1)S(1)} %slice.54), channel_id=1, source_target_pairs={{0,4},{4,8},{8,12},{12,16},{16,20},{20,24},{24,28},{1,5},{5,9},{9,... | collective-permute-start | bytes 3080 | tf_op jit(solution)/shard_map/ppermute | solution.py:24
  126.1 6.9 %collective-permute-start.4 = (bf16[128,256]{0,1:T(8,128)(2,1)S(1)}, bf16[128,256]{0,1:T(8,128)(2,1)}, u32[]{:S(2)}, u32[]{:S(2)}) collective-permute-start(bf16[128,256]{0,1:T(8,128)(2,1)S(1)} %collective-permute-done.3), channel_id=1, source_target_pairs={{0,8},{8,0},{4,12},{12,4},{16,24},{24,16},{20,28},{28,20},{1,9},{9... | collective-permute-start | bytes 196616 | tf_op jit(solution)/shard_map/ppermute | solution.py:18
  133.0 18.6 %collective-permute-start.5 = (bf16[128,256]{0,1:T(8,128)(2,1)}, bf16[128,256]{0,1:T(8,128)(2,1)S(1)}, u32[]{:S(2)}, u32[]{:S(2)}) collective-permute-start(bf16[128,256]{0,1:T(8,128)(2,1)} %collective-permute-done.4), channel_id=1, source_target_pairs={{0,16},{16,0},{4,20},{20,4},{8,24},{24,8},{12,28},{28,12},{1,17},{... | collective-permute-start | bytes 196616 | tf_op jit(solution)/shard_map/ppermute | solution.py:18
  133.1 2.1 %copy-start.13 = (bf16[2048,128]{1,0:T(8,128)(2,1)}, bf16[2048,128]{1,0:T(8,128)(2,1)S(1)}, u32[]{:S(2)}) copy-start(bf16[2048,128]{1,0:T(8,128)(2,1)S(1)} %get-tuple-element.462) | copy-start | bytes 1572868 | tf_op jit(solution)/shard_map/while
  133.1 2.1 %copy-start.15 = (bf16[128,1,2,128]{3,0,2,1:T(8,128)(2,1)}, bf16[128,1,2,128]{3,0,2,1:T(8,128)(2,1)S(1)}, u32[]{:S(2)}) copy-start(bf16[128,1,2,128]{3,0,2,1:T(8,128)(2,1)S(1)} %get-tuple-element.463) | copy-start | bytes 196612 | tf_op jit(solution)/shard_map/while
  137.7 1.2 copy-start.4
  138.2 2.3 %copy-start.6 = (bf16[2048,128]{0,1:T(8,128)(2,1)S(1)}, bf16[2048,128]{0,1:T(8,128)(2,1)}, u32[]{:S(2)}) copy-start(bf16[2048,128]{0,1:T(8,128)(2,1)} %get-tuple-element.461) | copy-start | bytes 1572868 | tf_op jit(solution)/shard_map/while
  139.0 1.7 copy-start.14
  139.0 1.8 copy-start.16
  156.6 3.6 %collective-permute-start.7 = (bf16[128,2]{0,1:T(2,128)(2,1)S(1)}, bf16[128,2]{0,1:T(2,128)(2,1)S(1)}, u32[]{:S(2)}, u32[]{:S(2)}) collective-permute-start(bf16[128,2]{0,1:T(2,128)(2,1)S(1)} %convert_bitcast_fusion), channel_id=1, source_target_pairs={{0,4},{4,0},{8,12},{12,8},{16,20},{20,16},{24,28},{28,24},{1,5},{5... | collective-permute-start | bytes 1544 | tf_op jit(solution)/shard_map/ppermute | solution.py:18
  160.3 3.6 %collective-permute-start.8 = (bf16[128,2]{0,1:T(2,128)(2,1)S(1)}, bf16[128,2]{0,1:T(2,128)(2,1)S(1)}, u32[]{:S(2)}, u32[]{:S(2)}) collective-permute-start(bf16[128,2]{0,1:T(2,128)(2,1)S(1)} %collective-permute-done.7), channel_id=1, source_target_pairs={{0,8},{8,0},{4,12},{12,4},{16,24},{24,16},{20,28},{28,20},{1,9},{9... | collective-permute-start | bytes 1544 | tf_op jit(solution)/shard_map/ppermute | solution.py:18
  163.9 4.5 %collective-permute-start.9 = (bf16[128,2]{0,1:T(2,128)(2,1)S(1)}, bf16[128,2]{0,1:T(2,128)(2,1)S(1)}, u32[]{:S(2)}, u32[]{:S(2)}) collective-permute-start(bf16[128,2]{0,1:T(2,128)(2,1)S(1)} %collective-permute-done.8), channel_id=1, source_target_pairs={{0,16},{16,0},{4,20},{20,4},{8,24},{24,8},{12,28},{28,12},{1,17},{... | collective-permute-start | bytes 1544 | tf_op jit(solution)/shard_map/ppermute | solution.py:18
Sparse Core Ops, SparseCore 0:
  9.6 25.2 all-gather.3
  37.0 63.7 all-gather.7
  102.9 48.6 all-gather.5
  156.8 29.6 reduce-scatter.1
